TPU v7x, 32 devices: a whole 2x2x4 slice. The times are simulated.
32 devices in a mesh: sp: 8 (over z, y), tp: 4 (over x, core).
Axes of the slice: x: 2, y: 2, z: 4, core: 2. Of those that a mesh axis runs over, the one named last changes fastest.
Arguments:
- residual: bfloat16 [3072, 2048], P(('sp', 'tp')), may hold values from -6 to 6
- query_one: bfloat16 [3072, 512], P('sp', 'tp'), may hold values from -6 to 6
- key_one: bfloat16 [3072, 512], P('sp', 'tp'), may hold values from -6 to 6
- value_one: bfloat16 [3072, 1024], P('sp', 'tp'), may hold values from -6 to 6
- gate_one: bfloat16 [3072, 1024], P('sp', 'tp'), may hold values from -6 to 6
- decay_one: bfloat16 [2, 3072, 512], P(None, 'sp', 'tp'), may hold values from -12 to 12
- norm_one: float32 [128], replicated, may hold values from 0.1 to 1.9
- output_one: bfloat16 [1024, 2048], P('tp'), may hold values from -0.125 to 0.125
- query_two: bfloat16 [3072, 1024], P('sp', 'tp'), may hold values from -6 to 6
- key_two: bfloat16 [3072, 1024], P('sp', 'tp'), may hold values from -6 to 6
- value_two: bfloat16 [3072, 1024], P('sp', 'tp'), may hold values from -6 to 6
- gate_two: bfloat16 [3072, 1024], P('sp', 'tp'), may hold values from -6 to 6
- decay_two: bfloat16 [2, 3072, 1024], P(None, 'sp', 'tp'), may hold values from -12 to 12
- norm_two: float32 [128], replicated, may hold values from 0.1 to 1.9
- output_two: bfloat16 [1024, 2048], P('tp'), may hold values from -0.125 to 0.125
- norm_gain: float32 [2048], replicated, may hold values from 0.1 to 1.9
- expert_ids: int32 [3072, 2], P('sp'), may hold values from 0 to 7, as said below
- group_weight: float32 [3072], P('sp'), may hold values from 0.25 to 1
- pair_weight: float32 [3072, 2], P('sp'), may hold values from 0.05 to 1
- expert_gate: bfloat16 [8, 2048, 1024], P('sp', None, 'tp'), may hold values from -0.125 to 0.125
- expert_up: bfloat16 [8, 2048, 1024], P('sp', None, 'tp'), may hold values from -0.125 to 0.125
- expert_down: bfloat16 [8, 1024, 2048], P('sp', 'tp'), may hold values from -0.1875 to 0.1875
Outputs:
- layer_out: bfloat16 [3072, 2048], P(('sp', 'tp'))
Inputs may be any that keep to these rules, and one draw needn't show every extreme that they name: `expert_ids`: each row names two different experts of one group, the group of expert e being e // 2. In each aligned block of 96 rows no expert is named more than 49 times, and one expert, the same in every block, is named exactly 49 times in each block.
All inputs are finite; a program needn't handle non-finite values.
Results may differ from a plain program's by a relative error of at most 0.018.
Values may be sent and summed in bfloat16 or wider, within the bound.
A program may use at most 128 MiB of HBM per device.

v0:
```python
import jax
import jax.numpy as jnp
from jax import lax
from jax.sharding import PartitionSpec as P

D = 2048
KEY_ONE = 64
KEY_TWO = 128
VALUE_W = 128
BLOCK = 64
GROUPS = 4


HIGH = lax.Precision.HIGHEST
TAU = 16.0
EPS = 1e-06


def prefix(array, axis, combine, identity, reverse):
    length, place = (lax.axis_size(axis), lax.axis_index(axis))
    everything = jax.tree.map(
        lambda part, kind: lax.all_gather(part.astype(kind), axis),
        array,
        (jnp.bfloat16, jnp.bfloat16, jnp.bfloat16, jnp.bfloat16),
    )
    start = jax.tree.map(
        lambda part, zero: jnp.broadcast_to(jnp.asarray(zero, part.dtype), part.shape),
        array,
        identity,
    )

    def turn(k, before):
        at = length - 1 - k if reverse else k
        reached = at > place if reverse else at < place
        new = combine(
            before, jax.tree.map(lambda part, own: part[at].astype(own.dtype), everything, array)
        )
        return jax.tree.map(lambda a, b: jnp.where(reached, a, b), new, before)

    return lax.fori_loop(0, length, turn, start)


def advance(state_now, step_input):
    fade_rate, extra_term = step_input
    return (fade_rate[..., None] * state_now + extra_term, state_now)


def rounded(term):
    return lax.optimization_barrier(term.astype(jnp.bfloat16)).astype(jnp.float32)


def slot_table(routes, capacity, experts):
    flat = routes.reshape(-1)
    count = flat.shape[0]
    onehot = (flat[:, None] == jnp.arange(experts, dtype=jnp.int32)[None, :]).astype(jnp.int32)
    place = jnp.sum((jnp.cumsum(onehot, axis=0) - onehot) * onehot, axis=1)
    table = (
        jnp.full((experts, capacity), count, jnp.int32)
        .at[flat, place]
        .set(jnp.arange(count, dtype=jnp.int32))
    )
    return (table, place)


def local_pass(queries, key_rows, values, rates):
    length, heads, width = queries.shape
    blocks = length // BLOCK
    shaped = (blocks, BLOCK, heads, width)
    cumul = jnp.cumsum(rates.reshape(shaped), axis=1)
    block_end = cumul[:, -1]
    key_blocks = key_rows.reshape(shaped)
    value_blocks = values.reshape(blocks, BLOCK, heads, values.shape[-1])
    query_dec = queries.reshape(shaped) * jnp.exp(cumul)
    query_low = query_dec.astype(jnp.bfloat16)
    key_dec = (key_blocks * jnp.exp(-cumul)).astype(jnp.bfloat16)
    key_end = (key_blocks * jnp.exp(block_end[:, None] - cumul)).astype(jnp.bfloat16)
    lower_mask = jnp.tril(jnp.ones((BLOCK, BLOCK), jnp.float32))
    scores = (
        jnp.einsum("nthd,nshd->nhts", query_low, key_dec, preferred_element_type=jnp.float32)
        * lower_mask
    )
    scores = scores.astype(jnp.bfloat16)
    inner_part = jnp.einsum(
        "nhts,nshe->nthe", scores, value_blocks, preferred_element_type=jnp.float32
    )
    added = jnp.einsum("nshd,nshe->nhde", key_end, value_blocks, preferred_element_type=jnp.float32)
    empty = jnp.zeros((heads, width, values.shape[-1]), jnp.float32)
    state_out, before = lax.scan(advance, empty, (jnp.exp(block_end), added))
    outer_part = jnp.einsum("nthd,nhde->nthe", query_dec, before, precision=HIGH)
    reach = jnp.cumsum(block_end, axis=0) - block_end
    query_reach = query_dec * jnp.exp(reach)[:, None]
    fade_total = jnp.exp(jnp.sum(block_end, axis=0))
    return (inner_part + outer_part, query_reach, fade_total, state_out)


def group_local(query, key_in, value, decay, width):
    heads = query.shape[1] // width
    queries = query.astype(jnp.float32).reshape(-1, heads, width) * width ** (-0.5)
    key_rows = key_in.astype(jnp.float32).reshape(-1, heads, width)
    values = value.reshape(-1, heads, VALUE_W)
    rates = jax.nn.log_sigmoid(decay.astype(jnp.float32)) / TAU
    ahead = local_pass(queries, key_rows, values, rates[0].reshape(-1, heads, width))
    behind = local_pass(
        jnp.flip(queries, 0),
        jnp.flip(key_rows, 0),
        jnp.flip(values, 0),
        jnp.flip(rates[1], 0).reshape(-1, heads, width),
    )
    return (ahead, behind)


def combine_states(earlier, later):
    return (
        earlier[0] * later[0],
        later[0][..., None] * earlier[1] + later[1],
        earlier[2] * later[2],
        later[2][..., None] * earlier[3] + later[3],
    )


def read_out(local, carried):
    output, query_reach, _, _ = local
    blocks, block, heads, _ = output.shape
    extra = jnp.einsum("nthd,hde->nthe", query_reach, carried, precision=HIGH)
    return (output + extra).reshape(blocks * block, heads, -1)


def finish(ahead_out, behind_out, gain, gate):
    total = ahead_out + jnp.flip(behind_out, 0)
    scale = lax.rsqrt(jnp.mean(total * total, axis=-1, keepdims=True) + EPS)
    normed = (total * scale * gain).reshape(total.shape[0], -1)
    return (normed * jax.nn.silu(gate.astype(jnp.float32))).astype(jnp.bfloat16)


def body(
    residual,
    query_one,
    key_one,
    value_one,
    gate_one,
    decay_one,
    norm_one,
    output_one,
    query_two,
    key_two,
    value_two,
    gate_two,
    decay_two,
    norm_two,
    output_two,
    norm_gain,
    expert_ids,
    group_weight,
    pair_weight,
    expert_gate,
    expert_up,
    expert_down,
):
    ahead_one, behind_one = group_local(query_one, key_one, value_one, decay_one, KEY_ONE)
    ahead_two, behind_two = group_local(query_two, key_two, value_two, decay_two, KEY_TWO)
    identity = (
        jnp.ones_like(ahead_one[2]),
        jnp.zeros_like(ahead_one[3]),
        jnp.ones_like(ahead_two[2]),
        jnp.zeros_like(ahead_two[3]),
    )
    carried_ahead = prefix(
        (ahead_one[2], ahead_one[3], ahead_two[2], ahead_two[3]),
        "sp",
        combine_states,
        identity,
        False,
    )
    carried_behind = prefix(
        (behind_one[2], behind_one[3], behind_two[2], behind_two[3]),
        "sp",
        combine_states,
        identity,
        True,
    )
    mixed_one = finish(
        read_out(ahead_one, carried_ahead[1]),
        read_out(behind_one, carried_behind[1]),
        norm_one,
        gate_one,
    )
    mixed_two = finish(
        read_out(ahead_two, carried_ahead[3]),
        read_out(behind_two, carried_behind[3]),
        norm_two,
        gate_two,
    )
    rows_dev = residual.shape[0]
    summed = lax.psum_scatter(
        (
            jnp.dot(mixed_one, output_one, preferred_element_type=jnp.float32)
            + jnp.dot(mixed_two, output_two, preferred_element_type=jnp.float32)
        ).astype(jnp.bfloat16),
        "tp",
        scatter_dimension=0,
        tiled=True,
    ).astype(jnp.float32)
    stream = (residual.astype(jnp.float32) + rounded(summed)).astype(jnp.bfloat16)
    wide = stream.astype(jnp.float32)
    normed_rows = (
        wide * lax.rsqrt(jnp.mean(wide * wide, axis=-1, keepdims=True) + EPS) * norm_gain
    ).astype(jnp.bfloat16)
    rank = lax.axis_index("tp")
    experts = lax.axis_size("sp")
    capacity = max(2, 2 * rows_dev // (experts - GROUPS) + 1)
    own_routes = lax.dynamic_slice_in_dim(expert_ids, rank * rows_dev, rows_dev, 0)
    own_group = lax.dynamic_slice_in_dim(group_weight, rank * rows_dev, rows_dev, 0)
    own_pair = lax.dynamic_slice_in_dim(pair_weight, rank * rows_dev, rows_dev, 0)
    weights = own_group[:, None] * own_pair / jnp.sum(own_pair, axis=1, keepdims=True)
    blank = jnp.zeros((1, D), jnp.bfloat16)
    table, own_place = slot_table(own_routes, capacity, experts)
    index = jnp.where(table == 2 * rows_dev, rows_dev, table // 2)
    send = jnp.concatenate([normed_rows, blank], axis=0)[index][None]
    received = lax.all_to_all(send, "sp", split_axis=1, concat_axis=1, tiled=True)
    received = lax.all_gather(received, "tp", axis=0, tiled=True)
    flat = received.reshape(-1, received.shape[-1])
    gate_part = jnp.dot(flat, expert_gate[0], preferred_element_type=jnp.float32)
    up_part = jnp.dot(flat, expert_up[0], preferred_element_type=jnp.float32)
    hidden = (jax.nn.silu(gate_part) * up_part).astype(jnp.bfloat16)
    share_sum = lax.psum_scatter(
        jnp.dot(hidden, expert_down[0], preferred_element_type=jnp.float32)
        .reshape(received.shape)
        .astype(jnp.bfloat16),
        "tp",
        scatter_dimension=0,
        tiled=True,
    )
    returned = lax.all_to_all(share_sum, "sp", split_axis=1, concat_axis=1, tiled=True)
    slot_index = own_routes.reshape(-1) * capacity + own_place
    picked = returned.reshape(-1, D)[slot_index].astype(jnp.float32).reshape(rows_dev, 2, D)
    layer = stream.astype(jnp.float32) + jnp.sum(weights[:, :, None] * picked, axis=1)
    return layer.astype(jnp.bfloat16)


def solution(mesh):
    placed = (
        P(("sp", "tp"), None),
        P("sp", "tp"),
        P("sp", "tp"),
        P("sp", "tp"),
        P("sp", "tp"),
        P(None, "sp", "tp"),
        P(),
        P("tp", None),
        P("sp", "tp"),
        P("sp", "tp"),
        P("sp", "tp"),
        P("sp", "tp"),
        P(None, "sp", "tp"),
        P(),
        P("tp", None),
        P(),
        P("sp", None),
        P("sp"),
        P("sp", None),
        P("sp", None, "tp"),
        P("sp", None, "tp"),
        P("sp", "tp", None),
    )
    return jax.shard_map(
        body, mesh=mesh, in_specs=placed, out_specs=P(("sp", "tp"), None), check_vma=False
    )
```

profile of v0, /device:TPU:0, one launch (start us, length us, event | category | flops | bytes accessed | tf_op | source)
XLA Modules:
  0.0 675.0 jit_solution(16346986232906719492)
XLA Ops:
  28.3 2.6 rev.39
  38.3 1.9 mul.387
  40.2 1.9 reshape_reshape.18
  42.1 2.7 multiply_convert_fusion.7
  45.9 9.9 %while.86 = (s32[]{:T(128)}, f32[2,64,128]{2,1,0:T(8,128)S(1)}, f32[6,2,64,128]{3,2,1,0:T(8,128)S(1)}, f32[6,2,64]{2,1,0:T(2,128)}, f32[6,2,64,128]{3,2,1,0:T(8,128)}, /*index=5*/s32[]{:T(128)}, s32[]{:T(128)}) while((s32[]{:T(128)}, f32[2,64,128]{2,1,0:T(8,128)S(1)}, f32[6,2,64,128]{3,2,1,0:T(8,128)S(1)}, f32[6,2,64]{2,1,0:T(2,128)}, ...), condition=%wide.region_2.3_spmd.clone, body=%wide.region_1.2_spmd.clone.sunk | while | flops 65539 | bytes 329316 | solution.py:88
  55.8 34.6 %all-gather.1 = bf16[16,64,128]{2,1,0:T(8,128)(2,1)} all-gather(bf16[2,64,128]{2,1,0:T(8,128)(2,1)S(1)} %convert_element_type.301), channel_id=3, replica_groups=mesh['sp'=8,'tp'=4] {'sp'}, dimensions={0}, use_global_device_ids=true | all-gather | bytes 294912 | tf_op jit(solution)/shard_map/all_gather | solution.py:22
  90.4 1.9 mul.415
  92.3 2.5 multiply_convert_fusion.1
  96.0 10.4 %while.87 = (s32[]{:T(128)}, f32[2,128,128]{2,1,0:T(8,128)S(1)}, f32[6,2,128,128]{3,2,1,0:T(8,128)S(1)}, f32[6,2,128]{2,1,0:T(2,128)}, f32[6,2,128,128]{3,2,1,0:T(8,128)}, /*index=5*/s32[]{:T(128)}, s32[]{:T(128)}) while((s32[]{:T(128)}, f32[2,128,128]{2,1,0:T(8,128)S(1)}, f32[6,2,128,128]{3,2,1,0:T(8,128)S(1)}, ...), condition=%wide.region_7.8_spmd.clone, body=%wide.region_6.7_spmd.clone.sunk | while | flops 131075 | bytes 658532 | solution.py:88
  106.5 33.2 %all-gather.3 = bf16[16,128,128]{2,1,0:T(8,128)(2,1)} all-gather(bf16[2,128,128]{2,1,0:T(8,128)(2,1)S(1)} %convert_element_type.307), channel_id=5, replica_groups=mesh['sp'=8,'tp'=4] {'sp'}, dimensions={0}, use_global_device_ids=true | all-gather | bytes 589824 | tf_op jit(solution)/shard_map/all_gather | solution.py:22
  140.4 20.9 %all-gather.9 = bf16[8,2,128]{2,1,0:T(2,128)(2,1)S(1)} all-gather(bf16[1,2,128]{2,1,0:T(2,128)(2,1)S(1)} %fusion.115), channel_id=4, replica_groups=mesh['sp'=8,'tp'=4] {'sp'}, dimensions={0}, use_global_device_ids=true | all-gather | bytes 4608 | tf_op jit(solution)/shard_map/all_gather | solution.py:22
  161.9 16.3 %all-gather.8 = bf16[8,2,64]{2,1,0:T(2,128)(2,1)S(1)} all-gather(bf16[1,2,64]{2,1,0:T(2,128)(2,1)S(1)} %fusion.114), channel_id=2, replica_groups=mesh['sp'=8,'tp'=4] {'sp'}, dimensions={0}, use_global_device_ids=true | all-gather | bytes 2304 | tf_op jit(solution)/shard_map/all_gather | solution.py:22
  178.2 15.2 %while.88 = (s32[]{:T(128)}, f32[2,64,128]{2,1,0:T(8,128)S(1)}, f32[2,128,128]{2,1,0:T(8,128)S(1)}, s32[]{:T(128)}, bf16[8,2,64]{2,1,0:T(2,128)(2,1)S(1)}, /*ind...) while((s32[]{:T(128)}, f32[2,64,128]{2,1,0:T(8,128)S(1)}, ...), condition=%wide.region_9.10_spmd.clone, body=%wide.region_8.9_spmd.clone.sunk | while | flops 246148 | bytes 495499 | solution.py:40
  195.5 2.2 convolution_bitcast_fusion.5
  202.9 2.6 multiply_convert_fusion.4
  207.3 13.5 %while.89 = (s32[]{:T(128)}, f32[2,64,128]{2,1,0:T(8,128)S(1)}, f32[6,2,64,128]{3,2,1,0:T(8,128)}, f32[6,2,64]{2,1,0:T(2,128)}, f32[6,2,64,128]{3,2,1,0:T(8,128)}, /*index=5*/s32[]{:T(128)}, s32[]{:T(128)}) while((s32[]{:T(128)}, f32[2,64,128]{2,1,0:T(8,128)S(1)}, f32[6,2,64,128]{3,2,1,0:T(8,128)}, f32[6,2,64]{2,1,0:T(2,128)}, ...), condition=%wide.region_13.14_spmd.clone, body=%wide.region_12.13_spmd.clone.sunk | while | flops 65539 | bytes 329824 | solution.py:88
  220.9 32.9 %all-gather.5 = bf16[16,64,128]{2,1,0:T(8,128)(2,1)} all-gather(bf16[2,64,128]{2,1,0:T(8,128)(2,1)S(1)} %convert_element_type.314), channel_id=7, replica_groups=mesh['sp'=8,'tp'=4] {'sp'}, dimensions={0}, use_global_device_ids=true | all-gather | bytes 294912 | tf_op jit(solution)/shard_map/all_gather | solution.py:22
  254.7 2.0 reverse_multiply_fusion
  256.7 2.7 rev.41
  259.6 2.7 multiply_convert_fusion
  264.4 14.2 %while.90 = (s32[]{:T(128)}, f32[2,128,128]{2,1,0:T(8,128)S(1)}, f32[6,2,128,128]{3,2,1,0:T(8,128)}, f32[6,2,128]{2,1,0:T(2,128)}, f32[6,2,128,128]{3,2,1,0:T(8,128)}, /*index=5*/s32[]{:T(128)}, s32[]{:T(128)}) while((s32[]{:T(128)}, f32[2,128,128]{2,1,0:T(8,128)S(1)}, f32[6,2,128,128]{3,2,1,0:T(8,128)}, ...), condition=%wide.region_18.19_spmd.clone, body=%wide.region_17.18_spmd.clone.sunk | while | flops 131075 | bytes 659040 | solution.py:88
  278.7 33.2 %all-gather.7 = bf16[16,128,128]{2,1,0:T(8,128)(2,1)} all-gather(bf16[2,128,128]{2,1,0:T(8,128)(2,1)S(1)} %convert_element_type.318), channel_id=9, replica_groups=mesh['sp'=8,'tp'=4] {'sp'}, dimensions={0}, use_global_device_ids=true | all-gather | bytes 589824 | tf_op jit(solution)/shard_map/all_gather | solution.py:22
  311.9 18.3 %all-gather.11 = bf16[8,2,128]{2,1,0:T(2,128)(2,1)S(1)} all-gather(bf16[1,2,128]{2,1,0:T(2,128)(2,1)S(1)} %fusion.117), channel_id=8, replica_groups=mesh['sp'=8,'tp'=4] {'sp'}, dimensions={0}, use_global_device_ids=true | all-gather | bytes 4608 | tf_op jit(solution)/shard_map/all_gather | solution.py:22
  330.2 16.3 %all-gather.10 = bf16[8,2,64]{2,1,0:T(2,128)(2,1)S(1)} all-gather(bf16[1,2,64]{2,1,0:T(2,128)(2,1)S(1)} %fusion.116), channel_id=6, replica_groups=mesh['sp'=8,'tp'=4] {'sp'}, dimensions={0}, use_global_device_ids=true | all-gather | bytes 2304 | tf_op jit(solution)/shard_map/all_gather | solution.py:22
  346.4 15.2 %while.91 = (s32[]{:T(128)}, f32[2,64,128]{2,1,0:T(8,128)S(1)}, f32[2,128,128]{2,1,0:T(8,128)S(1)}, s32[]{:T(128)}, bf16[8,2,64]{2,1,0:T(2,128)(2,1)S(1)}, /*ind...) while((s32[]{:T(128)}, f32[2,64,128]{2,1,0:T(8,128)S(1)}, ...), condition=%wide.region_20.21_spmd.clone, body=%wide.region_19.20_spmd.clone.sunk | while | flops 246152 | bytes 495561 | solution.py:40
  363.1 2.1 convolution_bitcast_fusion.2
  365.2 2.2 fusion.20
  368.8 2.0 copy.174
  373.4 2.2 convolution_bitcast_fusion.10
  382.3 1.9 fusion.130
  388.3 9.3 %scatter_fusion = s32[8,49]{1,0:T(8,128)S(1)} fusion(s32[8,49]{1,0:T(8,128)S(1)} %broadcast.166, s32[192]{0:T(256)S(1)} %bitcast.262, s32[192]{0:T(256)S(1)} %iota.52), kind=kCustom, calls=%fused_computation.2 | custom fusion | bytes 3840 | tf_op jit(solution)/shard_map/scatter | solution.py:60
  397.7 15.3 %reduce-scatter.3.cloned.1.call-done = bf16[96,2048]{1,0:T(8,128)(2,1)} async-done(((bf16[384,2048]{1,0:T(8,128)(2,1)}), bf16[96,2048]{1,0:T(8,128)(2,1)}) %reduce-scatter.3.cloned.1.call-update) | async-done | bytes 393232 | tf_op jit(solution)/shard_map/reduce_scatter | solution.py:194
  415.4 2.5 gather_fusion
  419.6 48.0 %all_to_all.10 = bf16[1,8,49,2048]{3,2,0,1:T(8,128)(2,1)S(1)} all-to-all(bf16[1,8,49,2048]{3,2,0,1:T(8,128)(2,1)} %bitcast.263), channel_id=1, replica_groups=mesh['sp'=8,'tp'=4] {'sp'}, dimensions={1} | all-to-all | bytes 3211264 | tf_op jit(solution)/shard_map/all_to_all | solution.py:219
  467.6 2.1 copy.180
  469.9 45.1 %all-gather.14.cloned.1.call-done = bf16[4,8,49,2048]{3,1,2,0:T(8,128)(2,1)} async-done(((bf16[1,8,49,2048]{3,1,2,0:T(8,128)(2,1)}), bf16[4,8,49,2048]{3,1,2,0:T(8,128)(2,1)}) %all-gather.14.cloned.1.call-update) | async-done | bytes 6422544 | tf_op jit(solution)/shard_map/all_gather | solution.py:220
  515.0 9.6 %copy.181 = bf16[4,8,49,2048]{3,2,1,0:T(8,128)(2,1)} copy(bf16[4,8,49,2048]{3,1,2,0:T(8,128)(2,1)} %all-gather.14.cloned.1.call-done) | data formatting | bytes 12845056 | tf_op jit(solution)/shard_map/all_gather | solution.py:220
  524.6 7.1 %reshape.334 = bf16[1568,2048]{1,0:T(8,128)(2,1)} reshape(bf16[4,8,49,2048]{3,2,1,0:T(8,128)(2,1)} %copy.181) | data formatting | bytes 12845056 | tf_op jit(solution)/shard_map/reshape | solution.py:221
  531.7 4.9 fusion.35
  536.6 2.1 fusion.12
  539.0 5.0 convolution_convert_fusion
  544.1 66.1 %reduce-scatter.5.cloned.1.call-done = bf16[1,8,49,2048]{3,2,1,0:T(8,128)(2,1)} async-done(((bf16[4,8,49,2048]{3,2,1,0:T(8,128)(2,1)}), bf16[1,8,49,2048]{3,2,1,0:T(8,128)(2,1)}) %reduce-scatter.5.cloned.1.call-update) | async-done | bytes 1605648 | tf_op jit(solution)/shard_map/reduce_scatter | solution.py:225
  610.2 6.0 all-to-all-start.1
  617.2 41.4 %all-to-all-done.1 = bf16[1,8,49,2048]{3,2,0,1:T(8,128)(2,1)} async-done(((bf16[1,8,49,2048]{3,2,0,1:T(8,128)(2,1)}), bf16[1,8,49,2048]{3,2,0,1:T(8,128)(2,1)}, u32[]{:S(2)}, u32[]{:S(2)}) %all-to-all-start.1) | async-done | bytes 1605664 | tf_op jit(solution)/shard_map/all_to_all | solution.py:233
  658.6 2.0 reshape.335
  660.6 2.0 gather_fusion.1
  662.7 2.2 reshape.345
  664.9 2.3 multiply_reduce_fusion
  (365 shorter events, 144.6 us)
Async XLA Ops:
  6.5 532.5 %copy-start = (bf16[1,256,2048]{2,1,0:T(8,128)(2,1)S(1)}, bf16[1,256,2048]{2,1,0:T(8,128)(2,1)}, u32[]{:S(2)}) copy-start(bf16[1,256,2048]{2,1,0:T(8,128)(2,1)} %param.55) | copy-start | bytes 3145732
  6.5 4.1 copy-start.31
  6.5 406.4 %reduce-scatter.3.cloned.1.call-start = ((), (), s32[]{:S(2)}) async-start(), calls=%async_computation.4 | async-start | bytes 1966080 | tf_op jit(solution)/shard_map/reduce_scatter | solution.py:194
  12.1 7.4 %copy-start.24 = (bf16[384,256]{1,0:T(8,128)(2,1)S(1)}, bf16[384,256]{1,0:T(8,128)(2,1)}, u32[]{:S(2)}) copy-start(bf16[384,256]{1,0:T(8,128)(2,1)} %param.37) | copy-start | bytes 589828
  15.7 7.2 %copy-start.29 = (bf16[384,256]{1,0:T(8,128)(2,1)S(1)}, bf16[384,256]{1,0:T(8,128)(2,1)}, u32[]{:S(2)}) copy-start(bf16[384,256]{1,0:T(8,128)(2,1)} %param.43) | copy-start | bytes 589828
  15.8 9.7 %copy-start.10 = (f32[6,64,2,64]{3,2,1,0:T(2,128)}, f32[6,64,2,64]{3,2,1,0:T(2,128)S(1)}, u32[]{:S(2)}) copy-start(f32[6,64,2,64]{3,2,1,0:T(2,128)S(1)} %fusion.128) | copy-start | bytes 589828
  18.0 9.4 %copy-start.25 = (bf16[384,256]{1,0:T(8,128)(2,1)S(1)}, bf16[384,256]{1,0:T(8,128)(2,1)}, u32[]{:S(2)}) copy-start(bf16[384,256]{1,0:T(8,128)(2,1)} %param.44) | copy-start | bytes 589828
  19.6 25.2 %copy-start.7 = (bf16[6,64,2,128]{3,2,1,0:T(2,128)(2,1)}, bf16[6,64,2,128]{3,2,1,0:T(2,128)(2,1)S(1)}, u32[]{:S(2)}) copy-start(bf16[6,64,2,128]{3,2,1,0:T(2,128)(2,1)S(1)} %reshape_reshape.19) | copy-start | bytes 589828
  30.9 11.3 %copy-start.33 = (f32[6,2,64]{2,1,0:T(2,128)S(1)}, f32[6,2,64]{2,1,0:T(2,128)}, u32[]{:S(2)}) copy-start(f32[6,2,64]{2,1,0:T(2,128)} %fusion.32) | copy-start | bytes 9220
  30.9 11.2 %copy-start.36 = (f32[6,2,64]{2,1,0:T(2,128)S(1)}, f32[6,2,64]{2,1,0:T(2,128)}, u32[]{:S(2)}) copy-start(f32[6,2,64]{2,1,0:T(2,128)} %get-tuple-element.691) | copy-start | bytes 9220
  33.0 9.1 %copy-start.9 = (f32[6,64,2,128]{3,2,1,0:T(2,128)}, f32[6,64,2,128]{3,2,1,0:T(2,128)S(1)}, u32[]{:S(2)}) copy-start(f32[6,64,2,128]{3,2,1,0:T(2,128)S(1)} %fusion.129) | copy-start | bytes 1179652
  35.8 9.0 %copy-start.20 = (bf16[384,128]{0,1:T(8,128)(2,1)}, bf16[384,128]{0,1:T(8,128)(2,1)S(1)}, u32[]{:S(2)}) copy-start(bf16[384,128]{0,1:T(8,128)(2,1)S(1)} %copy.130) | copy-start | bytes 294916
  45.8 46.5 %copy-start.15 = (f32[6,64,2,128]{3,2,1,0:T(2,128)S(1)}, f32[6,64,2,128]{3,2,1,0:T(2,128)}, u32[]{:S(2)}) copy-start(f32[6,64,2,128]{3,2,1,0:T(2,128)} %reshape_reshape.20) | copy-start | bytes 1179652
  55.8 36.5 %copy-start.17 = (f32[6,2,64,128]{3,2,1,0:T(8,128)}, f32[6,2,64,128]{3,2,1,0:T(8,128)S(1)}, u32[]{:S(2)}) copy-start(f32[6,2,64,128]{3,2,1,0:T(8,128)S(1)} %get-tuple-element.456) | copy-start | bytes 1179652
  178.2 17.3 %copy-start.22 = (f32[64,64]{1,0:T(8,128)S(1)}, f32[64,64]{1,0:T(8,128)}, u32[]{:S(2)}) copy-start(f32[64,64]{1,0:T(8,128)} %fusion.103) | copy-start | bytes 49156
  193.4 4.3 copy-start.5
  195.5 4.2 copy-start.21
  199.6 1.3 copy-start.27
  199.6 2.5 copy-start.26
  199.6 3.3 copy-start.11
  199.6 3.3 copy-start.35
  205.5 48.3 %copy-start.14 = (f32[384,2,128]{2,1,0:T(2,128)S(1)}, f32[384,2,128]{2,1,0:T(2,128)}, u32[]{:S(2)}) copy-start(f32[384,2,128]{2,1,0:T(2,128)} %reshape.320) | copy-start | bytes 1179652
  207.3 52.2 %copy-start.34 = (f32[6,2,128]{2,1,0:T(2,128)S(1)}, f32[6,2,128]{2,1,0:T(2,128)}, u32[]{:S(2)}) copy-start(f32[6,2,128]{2,1,0:T(2,128)} %get-tuple-element.696) | copy-start | bytes 18436
  264.4 47.4 %copy-start.40 = (f32[2,128]{1,0:T(2,128)S(1)}, f32[2,128]{1,0:T(2,128)}, u32[]{:S(2)}) copy-start(f32[2,128]{1,0:T(2,128)} %get-tuple-element.697) | copy-start | bytes 3076
  264.4 65.7 %copy-start.39 = (f32[2,64]{1,0:T(2,128)S(1)}, f32[2,64]{1,0:T(2,128)}, u32[]{:S(2)}) copy-start(f32[2,64]{1,0:T(2,128)} %get-tuple-element.698) | copy-start | bytes 1540
  264.4 82.0 %copy-start.4 = (f32[2,64,128]{2,1,0:T(8,128)S(1)}, f32[2,64,128]{2,1,0:T(8,128)}, u32[]{:S(2)}) copy-start(f32[2,64,128]{2,1,0:T(8,128)} %custom-call.8) | copy-start | bytes 196612
  365.2 2.6 copy-start.41
  367.8 7.8 %copy-start.8 = (bf16[6,64,2,128]{3,2,1,0:T(2,128)(2,1)S(1)}, bf16[6,64,2,128]{3,2,1,0:T(2,128)(2,1)}, u32[]{:S(2)}) copy-start(bf16[6,64,2,128]{3,2,1,0:T(2,128)(2,1)} %copy-done.7) | copy-start | bytes 589828
  367.8 7.8 %copy-start.23 = (f32[64,64]{1,0:T(8,128)S(1)}, f32[64,64]{1,0:T(8,128)}, u32[]{:S(2)}) copy-start(f32[64,64]{1,0:T(8,128)} %fusion.103) | copy-start | bytes 49156
  368.8 6.8 %copy-start.30 = (bf16[6,64,2,64]{3,2,1,0:T(2,128)(2,1)S(1)}, bf16[6,64,2,64]{3,2,1,0:T(2,128)(2,1)}, u32[]{:S(2)}) copy-start(bf16[6,64,2,64]{3,2,1,0:T(2,128)(2,1)} %get-tuple-element.680) | copy-start | bytes 294916
  370.8 6.3 copy-start.6
  370.8 6.3 copy-start.12
  377.1 1.4 copy-start.18
  377.6 2.7 copy-start.13
  380.3 1.0 copy-start.42
  380.8 1.1 copy-start.16
  380.9 1.1 copy-start.28
  382.3 1.9 copy-start.19
  386.0 26.9 %copy-start.2 = (bf16[96,2048]{1,0:T(8,128)(2,1)S(1)}, bf16[96,2048]{1,0:T(8,128)(2,1)}, u32[]{:S(2)}) copy-start(bf16[96,2048]{1,0:T(8,128)(2,1)} %param.34) | copy-start | bytes 1179652
  386.0 28.2 %copy-start.37 = (f32[2048]{0:T(1024)S(1)}, f32[2048]{0:T(1024)}, u32[]{:S(2)}) copy-start(f32[2048]{0:T(1024)} %param.49) | copy-start | bytes 24580
  386.0 129.0 %all-gather.14.cloned.1.call-start = ((), (), s32[]{:S(2)}) async-start(), calls=%async_computation.5 | async-start | bytes 8028160 | tf_op jit(solution)/shard_map/all_gather | solution.py:220
  469.7 140.5 %reduce-scatter.5.cloned.1.call-start = ((), (), s32[]{:S(2)}) async-start(), calls=%async_computation.6 | async-start | bytes 9175040 | tf_op jit(solution)/shard_map/reduce_scatter | solution.py:225
  524.6 7.1 %copy-start.43 = (bf16[1,2048,256]{2,1,0:T(8,128)(2,1)S(1)}, bf16[1,2048,256]{2,1,0:T(8,128)(2,1)}, u32[]{:S(2)}) copy-start(bf16[1,2048,256]{2,1,0:T(8,128)(2,1)} %param.53) | copy-start | bytes 3145732
  531.7 4.9 copy-start.1
  531.7 4.9 copy-start.44
  610.2 6.0 copy-start.38
  610.2 48.4 %all-to-all-start.1 = ((bf16[1,8,49,2048]{3,2,0,1:T(8,128)(2,1)}), bf16[1,8,49,2048]{3,2,0,1:T(8,128)(2,1)}, u32[]{:S(2)}, u32[]{:S(2)}) async-start(bf16[1,8,49,2048]{3,2,0,1:T(8,128)(2,1)} %bitcast.264), calls=%async_computation.3 | async-start | bytes 3670016 | tf_op jit(solution)/shard_map/all_to_all | solution.py:233
  662.7 4.5 copy-start.3
  (1 other events, 0.9 us)
Sparse Core Ops, SparseCore 0:
  386.1 26.7 reduce-scatter.2
  469.8 45.1 all-gather.13
  544.2 65.9 reduce-scatter.4
where the time goes:
time: 688 us; the launch traced here: 675 us
  blocking collectives  254 us (37%)
  waiting for transfers between devices  168 us (24%)
  other arithmetic  98.6 us (14%)
  local copies, waits for them, and re-layouts  95.2 us (14%)
  matrix products  37.5 us (5%)
  between operations  14.4 us (2%)
    all_gather x8, blocking collectives, prefix(): lax.all_gather(part.astype(kind), axis)  206 us
    reduce_scatter x1, waiting for transfers between devices, body(): lax.psum_scatter(jnp.dot(hidden, expert_down[0], preferred_element_type=j...  66.1 us
    all_to_all x1, blocking collectives, body(): lax.all_to_all(send, 'sp', split_axis=1, concat_axis=1, tiled=True)  48 us
    all_gather x1, waiting for transfers between devices, body(): received = lax.all_gather(received, 'tp', axis=0, tiled=True)  45.1 us
    all_to_all x1, waiting for transfers between devices, body(): lax.all_to_all(share_sum, 'sp', split_axis=1, concat_axis=1, tiled=True)  41.4 us
    select_n x32, other arithmetic, turn(): return jax.tree.map(lambda a, b: jnp.where(reached, a, b), new, before)  29.2 us
    add x24, other arithmetic, advance(): return (fade_rate[..., None] * state_now + extra_term, state_now)  23.4 us
    mul x24, local copies, waits for them, and re-layouts, advance(): return (fade_rate[..., None] * state_now + extra_term, state_now)  16 us
  transfers between devices with their start and end apart: 4, of which 4 were waited for; matrix products, arithmetic and copies ran while one was open for 2% of the time, Pallas kernels for 0%

commit v1 on v0

v1 whole, which is shorter than its diff:
```python
import functools

import jax
import jax.numpy as jnp
from jax import lax
from jax.experimental import pallas as pl
from jax.experimental.pallas import tpu as pltpu
from jax.sharding import PartitionSpec as P

D = 2048
KEY_ONE = 64
KEY_TWO = 128
VALUE_W = 128
BLOCK = 64
GROUPS = 4


MESH = pl.DeviceIdType.MESH
TAU = 16.0
EPS = 1e-06


def log_sigmoid(x):
    return jnp.minimum(x, 0.0) - jnp.log1p(jnp.exp(-jnp.abs(x)))


def contract(a, b, dims):
    return lax.dot_general(a, b, (dims, ((), ())), preferred_element_type=jnp.float32)


NN, NT, TN = ((1,), (0,)), ((1,), (1,)), ((0,), (0,))


def flip_bit(index, bit):
    return index + bit - 2 * bit * lax.rem(index // bit, 2)


def meet(peers):
    barrier = pltpu.get_barrier_semaphore()
    for peer in peers:
        pl.semaphore_signal(barrier, inc=1, device_id=peer, device_id_type=MESH)
    pl.semaphore_wait(barrier, len(peers))


def mixer_kernel(
    n_sp,
    n_tp,
    q1,
    k1,
    v1,
    g1,
    d1,
    q2,
    k2,
    v2,
    g2,
    d2,
    norm1,
    norm2,
    out1,
    out2,
    res,
    gain,
    stream_ref,
    normed_ref,
    cum,
    qd,
    kd,
    added,
    ends,
    sent,
    got,
    carried,
    total,
    mixed,
    part_send,
    part_got,
    st_send,
    st_recv,
    pt_send,
    pt_recv,
):
    sp, tp = lax.axis_index("sp"), lax.axis_index("tp")
    length = q1.shape[0]
    blocks = length // BLOCK
    lanes = 128
    units = []
    for q, k, v, g, d, norm, key in (
        (q1, k1, v1, g1, d1, norm1, KEY_ONE),
        (q2, k2, v2, g2, d2, norm2, KEY_TWO),
    ):
        per = lanes // key
        for at in range(q.shape[1] // lanes):
            units.append((q, k, v, g, d, norm, key, per, at))
    count = len(units)
    bits = [1 << r for r in range(n_tp.bit_length() - 1)]

    meet(
        [(lax.rem(sp + off, n_sp), tp) for off in range(1, n_sp)]
        + [(sp, flip_bit(tp, bit)) for bit in bits]
    )

    t_at = lax.broadcasted_iota(jnp.int32, (length, length), 0)
    s_at = lax.broadcasted_iota(jnp.int32, (length, length), 1)
    same = (t_at // BLOCK) == (s_at // BLOCK)
    for way in range(2):
        tri = jnp.where(same & ((s_at <= t_at) if way == 0 else (s_at >= t_at)), 1.0, 0.0).astype(
            jnp.bfloat16
        )
        for u, (q, k, v, g, d, norm, key, per, at) in enumerate(units):
            cols = slice(at * lanes, (at + 1) * lanes)
            rate = log_sigmoid(d[way, :, cols].astype(jnp.float32)) / TAU
            high = rate.astype(jnp.bfloat16)
            rest = rate - high.astype(jnp.float32)
            mid = rest.astype(jnp.bfloat16)
            low = (rest - mid.astype(jnp.float32)).astype(jnp.bfloat16)
            cum[u] = contract(tri, high, NN) + contract(tri, mid, NN) + contract(tri, low, NN)
            state = jnp.zeros((VALUE_W, lanes), jnp.float32)
            reach = jnp.zeros((1, lanes), jnp.float32)
            lane = lax.broadcasted_iota(jnp.int32, (VALUE_W, lanes), 1) // key
            for n in range(blocks) if way == 0 else range(blocks - 1, -1, -1):
                rows = slice(n * BLOCK, (n + 1) * BLOCK)
                c = cum[u, rows, :]
                e = c[BLOCK - 1 : BLOCK] if way == 0 else c[0:1]
                queries = q[rows, cols].astype(jnp.float32) * key ** (-0.5)
                keys = k[rows, cols].astype(jnp.float32)
                qd[way, u, rows, :] = (queries * jnp.exp(c)).astype(jnp.bfloat16)
                kd[way, u, rows, :] = (keys * jnp.exp(-c)).astype(jnp.bfloat16)
                end = (keys * jnp.exp(e - c)).astype(jnp.bfloat16)
                term = None
                for h in range(per):
                    head = at * per + h
                    value = v[rows, head * VALUE_W : (head + 1) * VALUE_W]
                    new = contract(value, end, TN)
                    term = new if term is None else jnp.where(lane == h, new, term)
                added[way, u, n] = term
                fade = jnp.exp(e)
                ends[way, u, n : n + 1, :] = fade
                state = state * fade + term
                reach = reach + e
            sent[way, u * VALUE_W : (u + 1) * VALUE_W, :] = state.astype(jnp.bfloat16)
            sent[way, count * VALUE_W + 16 * u : count * VALUE_W + 16 * (u + 1), :] = (
                jnp.broadcast_to(jnp.exp(reach), (16, lanes)).astype(jnp.bfloat16)
            )

    def state_copy(off):
        to = lax.rem(sp + off, n_sp)
        way = jnp.where(to > sp, 0, 1)
        return pltpu.make_async_remote_copy(
            src_ref=sent.at[way],
            dst_ref=got.at[off],
            send_sem=st_send.at[off],
            recv_sem=st_recv.at[off],
            device_id=(to, tp),
            device_id_type=MESH,
        )

    @pl.loop(1, n_sp)
    def _(off):
        state_copy(off).start()

    t_blk = lax.broadcasted_iota(jnp.int32, (BLOCK, BLOCK), 0)
    s_blk = lax.broadcasted_iota(jnp.int32, (BLOCK, BLOCK), 1)
    first = 0
    for u, (q, k, v, g, d, norm, key, per, at) in enumerate(units):
        lane = lax.broadcasted_iota(jnp.int32, (BLOCK, lanes), 1) // key
        for h in range(per):
            head = at * per + h
            for n in range(blocks):
                rows = slice(n * BLOCK, (n + 1) * BLOCK)
                scores = None
                for way in range(2):
                    queries = qd[way, u, rows, :]
                    if per > 1:
                        queries = jnp.where(lane == h, queries, jnp.zeros_like(queries))
                    one = contract(queries, kd[way, u, rows, :], NT)
                    one = jnp.where((s_blk <= t_blk) if way == 0 else (s_blk >= t_blk), one, 0.0)
                    scores = one if scores is None else scores + one
                value = v[rows, head * VALUE_W : (head + 1) * VALUE_W]
                total[first + h, rows, :] = contract(scores.astype(jnp.bfloat16), value, NN)
        first += per

    @pl.loop(1, n_sp)
    def _(off):
        state_copy(off).wait()

    carried[...] = jnp.zeros_like(carried)

    def fold(way, who):
        off = lax.rem(sp - who + n_sp, n_sp)
        for u in range(count):
            fade = got[off, count * VALUE_W + 16 * u : count * VALUE_W + 16 * (u + 1), :][0:1]
            state = got[off, u * VALUE_W : (u + 1) * VALUE_W, :]
            carried[way, u] = carried[way, u] * fade.astype(jnp.float32) + state.astype(jnp.float32)

    @pl.loop(0, sp)
    def _(who):
        fold(0, who)

    @pl.loop(0, n_sp - 1 - sp)
    def _(back):
        fold(1, n_sp - 1 - back)

    first = 0
    for u, (q, k, v, g, d, norm, key, per, at) in enumerate(units):
        lane = lax.broadcasted_iota(jnp.int32, (BLOCK, lanes), 1) // key
        for way in range(2):
            state = carried[way, u]
            for n in range(blocks) if way == 0 else range(blocks - 1, -1, -1):
                rows = slice(n * BLOCK, (n + 1) * BLOCK)
                low = state.astype(jnp.bfloat16)
                for h in range(per):
                    queries = qd[way, u, rows, :]
                    if per > 1:
                        queries = jnp.where(lane == h, queries, jnp.zeros_like(queries))
                    total[first + h, rows, :] += contract(queries, low, NT)
                state = state * ends[way, u, n : n + 1, :] + added[way, u, n]
        for h in range(per):
            head = at * per + h
            cols = slice(head * VALUE_W, (head + 1) * VALUE_W)
            x = total[first + h]
            y = x * lax.rsqrt(jnp.mean(x * x, axis=-1, keepdims=True) + EPS) * norm[...]
            gate = g[:, cols].astype(jnp.float32)
            y = y * (gate / (1.0 + jnp.exp(-gate)))
            mixed[:, (first + h) * VALUE_W : (first + h + 1) * VALUE_W] = y.astype(jnp.bfloat16)
        first += per

    rows_dev = res.shape[0]
    split = out1.shape[0]

    def project(mask):
        block = tp
        for bit in bits:
            if mask & bit:
                block = flip_bit(block, bit)
        rows = pl.ds(pl.multiple_of(block * rows_dev, 16), rows_dev)
        return contract(mixed[rows, :split], out1[...], NN) + contract(
            mixed[rows, split:], out2[...], NN
        )

    def part_copy(mask, bit):
        return pltpu.make_async_remote_copy(
            src_ref=part_send.at[mask],
            dst_ref=part_got.at[mask],
            send_sem=pt_send.at[mask],
            recv_sem=pt_recv.at[mask],
            device_id=(sp, flip_bit(tp, bit)),
            device_id_type=MESH,
        )

    low_bit = lambda m: m & -m
    order = sorted(range(1, n_tp), key=lambda m: (low_bit(m), -m))
    for mask in order:
        bit = low_bit(mask)
        value = project(mask)
        for earlier in bits:
            if earlier < bit:
                part_copy(mask | earlier, earlier).wait_recv()
                value = value + part_got[mask | earlier].astype(jnp.float32)
        part_send[mask] = value.astype(jnp.bfloat16)
        part_copy(mask, bit).start()
    value = project(0)
    for bit in bits:
        part_copy(bit, bit).wait_recv()
        value = value + part_got[bit].astype(jnp.float32)
    stream = (res[...].astype(jnp.float32) + value.astype(jnp.bfloat16).astype(jnp.float32)).astype(
        jnp.bfloat16
    )
    stream_ref[...] = stream
    wide = stream.astype(jnp.float32)
    scale = lax.rsqrt(jnp.mean(wide * wide, axis=-1, keepdims=True) + EPS)
    normed_ref[...] = (wide * scale * gain[...]).astype(jnp.bfloat16)
    for mask in order:
        part_copy(mask, low_bit(mask)).wait_send()


def mixer(n_sp, n_tp, args, residual, norm_gain):
    q1, k1, v1, g1, d1, norm1, out1, q2, k2, v2, g2, d2, norm2, out2 = args
    length = q1.shape[0]
    blocks = length // BLOCK
    count = (q1.shape[1] + q2.shape[1]) // 128
    heads = (v1.shape[1] + v2.shape[1]) // VALUE_W
    rows, width = residual.shape
    packed = count * (VALUE_W + 16)
    bf, f32 = jnp.bfloat16, jnp.float32
    vmem = pl.BlockSpec(memory_space=pltpu.VMEM)
    sem = pltpu.SemaphoreType.DMA
    return pl.pallas_call(
        functools.partial(mixer_kernel, n_sp, n_tp),
        out_shape=(jax.ShapeDtypeStruct((rows, width), bf),) * 2,
        in_specs=[vmem] * 16,
        out_specs=(vmem, vmem),
        scratch_shapes=[
            pltpu.VMEM((count, length, 128), f32),
            pltpu.VMEM((2, count, length, 128), bf),
            pltpu.VMEM((2, count, length, 128), bf),
            pltpu.VMEM((2, count, blocks, VALUE_W, 128), f32),
            pltpu.VMEM((2, count, -(-blocks // 8) * 8, 128), f32),
            pltpu.VMEM((2, packed, 128), bf),
            pltpu.VMEM((n_sp, packed, 128), bf),
            pltpu.VMEM((2, count, VALUE_W, 128), f32),
            pltpu.VMEM((heads, length, VALUE_W), f32),
            pltpu.VMEM((length, heads * VALUE_W), bf),
            pltpu.VMEM((n_tp, rows, width), bf),
            pltpu.VMEM((n_tp, rows, width), bf),
            sem((n_sp,)),
            sem((n_sp,)),
            sem((n_tp,)),
            sem((n_tp,)),
        ],
        compiler_params=pltpu.CompilerParams(
            collective_id=0, has_side_effects=True, vmem_limit_bytes=60 * 2**20
        ),
    )(
        q1, k1, v1, g1, d1, q2, k2, v2, g2, d2,
        norm1[None], norm2[None], out1, out2, residual, norm_gain[None],
    )


def slot_table(routes, capacity, experts):
    flat = routes.reshape(-1)
    count = flat.shape[0]
    onehot = (flat[:, None] == jnp.arange(experts, dtype=jnp.int32)[None, :]).astype(jnp.int32)
    place = jnp.sum((jnp.cumsum(onehot, axis=0) - onehot) * onehot, axis=1)
    table = (
        jnp.full((experts, capacity), count, jnp.int32)
        .at[flat, place]
        .set(jnp.arange(count, dtype=jnp.int32))
    )
    return (table, place)


def body(
    residual,
    query_one,
    key_one,
    value_one,
    gate_one,
    decay_one,
    norm_one,
    output_one,
    query_two,
    key_two,
    value_two,
    gate_two,
    decay_two,
    norm_two,
    output_two,
    norm_gain,
    expert_ids,
    group_weight,
    pair_weight,
    expert_gate,
    expert_up,
    expert_down,
):
    stream, normed_rows = mixer(
        lax.axis_size("sp"),
        lax.axis_size("tp"),
        (
            query_one, key_one, value_one, gate_one, decay_one, norm_one, output_one,
            query_two, key_two, value_two, gate_two, decay_two, norm_two, output_two,
        ),
        residual,
        norm_gain,
    )
    rows_dev = residual.shape[0]
    rank = lax.axis_index("tp")
    experts = lax.axis_size("sp")
    capacity = max(2, 2 * rows_dev // (experts - GROUPS) + 1)
    own_routes = lax.dynamic_slice_in_dim(expert_ids, rank * rows_dev, rows_dev, 0)
    own_group = lax.dynamic_slice_in_dim(group_weight, rank * rows_dev, rows_dev, 0)
    own_pair = lax.dynamic_slice_in_dim(pair_weight, rank * rows_dev, rows_dev, 0)
    weights = own_group[:, None] * own_pair / jnp.sum(own_pair, axis=1, keepdims=True)
    blank = jnp.zeros((1, D), jnp.bfloat16)
    table, own_place = slot_table(own_routes, capacity, experts)
    index = jnp.where(table == 2 * rows_dev, rows_dev, table // 2)
    send = jnp.concatenate([normed_rows, blank], axis=0)[index][None]
    received = lax.all_to_all(send, "sp", split_axis=1, concat_axis=1, tiled=True)
    received = lax.all_gather(received, "tp", axis=0, tiled=True)
    flat = received.reshape(-1, received.shape[-1])
    gate_part = jnp.dot(flat, expert_gate[0], preferred_element_type=jnp.float32)
    up_part = jnp.dot(flat, expert_up[0], preferred_element_type=jnp.float32)
    hidden = (jax.nn.silu(gate_part) * up_part).astype(jnp.bfloat16)
    share_sum = lax.psum_scatter(
        jnp.dot(hidden, expert_down[0], preferred_element_type=jnp.float32)
        .reshape(received.shape)
        .astype(jnp.bfloat16),
        "tp",
        scatter_dimension=0,
        tiled=True,
    )
    returned = lax.all_to_all(share_sum, "sp", split_axis=1, concat_axis=1, tiled=True)
    slot_index = own_routes.reshape(-1) * capacity + own_place
    picked = returned.reshape(-1, D)[slot_index].astype(jnp.float32).reshape(rows_dev, 2, D)
    layer = stream.astype(jnp.float32) + jnp.sum(weights[:, :, None] * picked, axis=1)
    return layer.astype(jnp.bfloat16)


def solution(mesh):
    placed = (
        P(("sp", "tp"), None),
        P("sp", "tp"),
        P("sp", "tp"),
        P("sp", "tp"),
        P("sp", "tp"),
        P(None, "sp", "tp"),
        P(),
        P("tp", None),
        P("sp", "tp"),
        P("sp", "tp"),
        P("sp", "tp"),
        P("sp", "tp"),
        P(None, "sp", "tp"),
        P(),
        P("tp", None),
        P(),
        P("sp", None),
        P("sp"),
        P("sp", None),
        P("sp", None, "tp"),
        P("sp", None, "tp"),
        P("sp", "tp", None),
    )
    return jax.shard_map(
        body, mesh=mesh, in_specs=placed, out_specs=P(("sp", "tp"), None), check_vma=False
    )
```

time: 688 us -> 324 us (0.47); the launches traced: 675 us -> 324 us
  blocking collectives: 254 us -> 53.1 us
  other arithmetic: 98.6 us -> 4.06 us
  local copies, waits for them, and re-layouts: 95.2 us -> 40.1 us
  Pallas kernels: 0 us -> 42 us
  matrix products: 37.5 us -> 12.1 us
  waiting for transfers between devices: 168 us -> 153 us
    all_gather x8 -> x0, blocking collectives: 206 us -> none  [prefix(): lax.all_gather(part.astype(kind), axis)]
    pallas_call x0 -> x1, Pallas kernels: none -> 42 us  [mixer(): pl.pallas_call(functools.partial(mixer_kernel, n_sp, n_tp), out_shape=(ja...]
    select_n x33 -> x0, other arithmetic: 29.9 us -> none  [the longest x32 29.2 us: turn(): return jax.tree.map(lambda a, b: jnp.where(reached, a, b), new, before)]
    dot_general x18 -> x0, matrix products: 25.4 us -> none  [the longest x4 7.1 us: local_pass(): jnp.einsum('nhts,nshe->nthe', scores, value_blocks, preferred_element_typ...]
    mul x29 -> x0, local copies, waits for them, and re-layouts: 23.8 us -> none  [the longest x24 16 us: advance(): return (fade_rate[..., None] * state_now + extra_term, state_now)]
    add x24 -> x0, other arithmetic: 23.4 us -> none  [advance(): return (fade_rate[..., None] * state_now + extra_term, state_now)]
    reduce_scatter x1 -> x0, waiting for transfers between devices: 15.3 us -> none  [body(): lax.psum_scatter((jnp.dot(mixed_one, output_one, preferred_element_type=j...]
    convert_element_type x46 -> x0, other arithmetic: 14.5 us -> none  [the longest x4 10.5 us: local_pass(): key_dec = (key_blocks * jnp.exp(-cumul)).astype(jnp.bfloat16)]
  transfers between devices with their start and end apart: 4 -> 3, of which waited for: 4 -> 3; matrix products, arithmetic and copies ran while one was open for 2% -> 0% of each run, Pallas kernels for 0% -> 0%
where the time goes in v1:
time: 324 us
  waiting for transfers between devices  153 us (47%)
  blocking collectives  53.1 us (16%)
  Pallas kernels  42 us (13%)
  local copies, waits for them, and re-layouts  40.1 us (12%)
  between operations  13.6 us (4%)
  matrix products  12.1 us (4%)
  starting transfers between devices  5.87 us (2%)
  other arithmetic  4.06 us (1%)
    reduce_scatter x1, waiting for transfers between devices, body(): lax.psum_scatter(jnp.dot(hidden, expert_down[0], preferred_element_type=j...  66.1 us
    all_to_all x1, blocking collectives, body(): lax.all_to_all(send, 'sp', split_axis=1, concat_axis=1, tiled=True)  53.1 us
    all_gather x1, waiting for transfers between devices, body(): received = lax.all_gather(received, 'tp', axis=0, tiled=True)  45.1 us
    pallas_call x1, Pallas kernels, mixer(): pl.pallas_call(functools.partial(mixer_kernel, n_sp, n_tp), out_shape=(ja...  42 us
    all_to_all x1, waiting for transfers between devices, body(): lax.all_to_all(share_sum, 'sp', split_axis=1, concat_axis=1, tiled=True)  41.5 us
    all_gather x1, local copies, waits for them, and re-layouts, body(): received = lax.all_gather(received, 'tp', axis=0, tiled=True)  9.59 us
    scatter x1, local copies, waits for them, and re-layouts, slot_table(): table = jnp.full((experts, capacity), count, jnp.int32).at[flat, place].s...  9.28 us
    reshape x1, local copies, waits for them, and re-layouts, body(): flat = received.reshape(-1, received.shape[-1])  7.08 us
  transfers between devices with their start and end apart: 3, of which 3 were waited for; matrix products, arithmetic and copies ran while one was open for 0% of the time, Pallas kernels for 0%

profile of v1, /device:TPU:0, one launch (start us, length us, event | category | flops | bytes accessed | tf_op | source)
XLA Modules:
  0.0 323.6 jit_solution(246420768256338208)
XLA Ops:
  6.5 0.0 copy-start
  6.5 0.0 all-gather.2.cloned.1.call-start
  6.5 0.8 constant_dynamic-slice_fusion
  7.4 0.1 copy.28
  7.5 0.1 eq.25
  7.6 0.1 reshape.98
  7.8 0.6 reduce-window.6
  8.4 0.2 slice_reduce_fusion
  8.6 0.1 add_bitcast_fusion
  8.8 9.3 %scatter_fusion = s32[8,49]{1,0:T(8,128)S(1)} fusion(s32[8,49]{1,0:T(8,128)S(1)} %broadcast.83, s32[192]{0:T(256)S(1)} %bitcast.32, s32[192]{0:T(256)S(1)} %iota.8), kind=kCustom, calls=%fused_computation.2 | custom fusion | bytes 3840 | tf_op jit(solution)/shard_map/scatter | solution.py:328
  18.1 0.1 reshape.107
  18.2 42.0 %shard_map.208 = (bf16[96,2048]{1,0:T(8,128)(2,1)}, bf16[96,2048]{1,0:T(8,128)(2,1)}) custom-call(bf16[384,128]{1,0:T(8,128)(2,1)} %q1.1, bf16[384,128]{1,0:T(8,128)(2,1)} %k1.1, bf16[384,256]{1,0:T(8,128)(2,1)} %v1.1, bf16[384,256]{1,0:T(8,128)(2,1)} %g1.1, bf16[2,384,128]{2,1,0:T(8,128)(2,1)} %d1.1, bf16[384,256]{1,0:T(8,128)(2,1)} %q2.1, ...), custom_call_target="tpu_custom_call" | custom-call | tf_op jit(solution)/shard_map/pallas_call | solution.py:288
  60.2 1.0 concatenate.6
  61.3 2.5 gather_fusion
  63.7 1.8 broadcast_in_dim.32
  65.5 53.1 %all_to_all.10 = bf16[1,8,49,2048]{3,2,0,1:T(8,128)(2,1)S(1)} all-to-all(bf16[1,8,49,2048]{3,2,0,1:T(8,128)(2,1)} %bitcast.33), channel_id=1, replica_groups=mesh['sp'=8,'tp'=4] {'sp'}, dimensions={1} | all-to-all | bytes 3211264 | tf_op jit(solution)/shard_map/all_to_all | solution.py:379
  118.6 2.1 copy.31
  120.6 0.0 all-gather.2.cloned.1.call-update
  120.7 0.2 reduce-scatter.2.cloned.1.call-start
  120.9 45.1 %all-gather.2.cloned.1.call-done = bf16[4,8,49,2048]{3,1,2,0:T(8,128)(2,1)} async-done(((bf16[1,8,49,2048]{3,1,2,0:T(8,128)(2,1)}), bf16[4,8,49,2048]{3,1,2,0:T(8,128)(2,1)}) %all-gather.2.cloned.1.call-update) | async-done | bytes 6422544 | tf_op jit(solution)/shard_map/all_gather | solution.py:380
  166.0 9.6 %copy.32 = bf16[4,8,49,2048]{3,2,1,0:T(8,128)(2,1)} copy(bf16[4,8,49,2048]{3,1,2,0:T(8,128)(2,1)} %all-gather.2.cloned.1.call-done) | data formatting | bytes 12845056 | tf_op jit(solution)/shard_map/all_gather | solution.py:380
  175.6 0.0 copy-start.4
  175.6 7.1 %reshape.101 = bf16[1568,2048]{1,0:T(8,128)(2,1)} reshape(bf16[4,8,49,2048]{3,2,1,0:T(8,128)(2,1)} %copy.32) | data formatting | bytes 12845056 | tf_op jit(solution)/shard_map/reshape | solution.py:381
  182.7 0.0 copy-done.4
  182.7 0.0 copy-start.1
  182.7 4.9 %fusion.3 = f32[1568,256]{1,0:T(8,128)S(1)} fusion(bf16[1568,2048]{1,0:T(8,128)(2,1)} %reshape.101, bf16[1,2048,256]{2,1,0:T(8,128)(2,1)S(1)} %copy-done.4), kind=kOutput, calls=%fused_computation.9 | convolution fusion | flops 1644167168 | bytes 9076736 | tf_op jit(solution)/shard_map/dot_general | solution.py:382
  187.6 0.0 copy-done.1
  187.6 0.0 copy-done.5
  187.6 2.1 fusion
  189.8 0.3 dot_general.13
  190.0 0.0 copy-done
  190.0 5.1 %convolution_convert_fusion = bf16[4,8,49,2048]{3,2,1,0:T(8,128)(2,1)} fusion(bf16[4,8,49,256]{3,2,1,0:T(8,128)(2,1)S(1)} %dot_general.13, bf16[1,256,2048]{2,1,0:T(8,128)(2,1)S(1)} %copy-done), kind=kOutput, calls=%fused_computation.3 | convolution fusion | flops 1647378432 | bytes 8273920 | tf_op jit(solution)/shard_map/dot_general | solution.py:386
  195.1 0.0 reduce-scatter.2.cloned.1.call-update
  195.1 66.1 %reduce-scatter.2.cloned.1.call-done = bf16[1,8,49,2048]{3,2,1,0:T(8,128)(2,1)} async-done(((bf16[4,8,49,2048]{3,2,1,0:T(8,128)(2,1)}), bf16[1,8,49,2048]{3,2,1,0:T(8,128)(2,1)}) %reduce-scatter.2.cloned.1.call-update) | async-done | bytes 1605648 | tf_op jit(solution)/shard_map/reduce_scatter | solution.py:385
  261.2 5.7 %all-to-all-start.1 = ((bf16[1,8,49,2048]{3,2,0,1:T(8,128)(2,1)}), bf16[1,8,49,2048]{3,2,0,1:T(8,128)(2,1)}, u32[]{:S(2)}, u32[]{:S(2)}) async-start(bf16[1,8,49,2048]{3,2,0,1:T(8,128)(2,1)} %bitcast.34), calls=%async_computation.2 | async-start | bytes 3670016 | tf_op jit(solution)/shard_map/all_to_all | solution.py:393
  266.9 0.0 copy-done.3
  266.9 0.1 dynamic-slice_reduce_fusion
  267.0 0.8 dynamic_slice.9
  267.7 0.1 multiply_divide_fusion
  267.8 0.1 copy.27
  267.9 41.5 %all-to-all-done.1 = bf16[1,8,49,2048]{3,2,0,1:T(8,128)(2,1)} async-done(((bf16[1,8,49,2048]{3,2,0,1:T(8,128)(2,1)}), bf16[1,8,49,2048]{3,2,0,1:T(8,128)(2,1)}, u32[]{:S(2)}, u32[]{:S(2)}) %all-to-all-start.1) | async-done | bytes 1605664 | tf_op jit(solution)/shard_map/all_to_all | solution.py:393
  309.4 2.0 reshape.102
  311.5 1.1 gather_fusion.1
  312.6 1.0 reshape.104
  313.6 0.0 copy-start.2
  313.6 2.3 multiply_reduce_fusion
  315.9 0.0 copy-done.2
  315.9 0.8 add_convert_fusion
  (13 shorter events, 0.1 us)
Async XLA Ops:
  6.5 183.5 %copy-start = (bf16[1,256,2048]{2,1,0:T(8,128)(2,1)S(1)}, bf16[1,256,2048]{2,1,0:T(8,128)(2,1)}, u32[]{:S(2)}) copy-start(bf16[1,256,2048]{2,1,0:T(8,128)(2,1)} %param.43) | copy-start | bytes 3145732
  6.5 159.5 %all-gather.2.cloned.1.call-start = ((), (), s32[]{:S(2)}) async-start(), calls=%async_computation.3 | async-start | bytes 8028160 | tf_op jit(solution)/shard_map/all_gather | solution.py:380
  120.7 140.6 %reduce-scatter.2.cloned.1.call-start = ((), (), s32[]{:S(2)}) async-start(), calls=%async_computation.4 | async-start | bytes 9175040 | tf_op jit(solution)/shard_map/reduce_scatter | solution.py:385
  175.6 7.1 %copy-start.4 = (bf16[1,2048,256]{2,1,0:T(8,128)(2,1)S(1)}, bf16[1,2048,256]{2,1,0:T(8,128)(2,1)}, u32[]{:S(2)}) copy-start(bf16[1,2048,256]{2,1,0:T(8,128)(2,1)} %param.41) | copy-start | bytes 3145732
  182.7 4.9 %copy-start.1 = (bf16[1568,2048]{1,0:T(8,128)(2,1)S(1)}, bf16[1568,2048]{1,0:T(8,128)(2,1)}, u32[]{:S(2)}) copy-start(bf16[1568,2048]{1,0:T(8,128)(2,1)} %reshape.101) | copy-start | bytes 19267588
  182.7 4.9 %copy-start.5 = (bf16[1,2048,256]{2,1,0:T(8,128)(2,1)S(1)}, bf16[1,2048,256]{2,1,0:T(8,128)(2,1)}, u32[]{:S(2)}) copy-start(bf16[1,2048,256]{2,1,0:T(8,128)(2,1)} %param.42) | copy-start | bytes 3145732
  261.2 5.7 %copy-start.3 = (f32[384,2]{0,1:T(2,128)S(1)}, f32[384,2]{0,1:T(2,128)}, u32[]{:S(2)}) copy-start(f32[384,2]{0,1:T(2,128)} %param.40) | copy-start | bytes 9220
  261.2 48.2 %all-to-all-start.1 = ((bf16[1,8,49,2048]{3,2,0,1:T(8,128)(2,1)}), bf16[1,8,49,2048]{3,2,0,1:T(8,128)(2,1)}, u32[]{:S(2)}, u32[]{:S(2)}) async-start(bf16[1,8,49,2048]{3,2,0,1:T(8,128)(2,1)} %bitcast.34), calls=%async_computation.2 | async-start | bytes 3670016 | tf_op jit(solution)/shard_map/all_to_all | solution.py:393
  313.6 2.3 copy-start.2
Sparse Core Ops, SparseCore 0:
  120.8 45.2 all-gather.1
  195.2 65.9 reduce-scatter.1

commit v2 on v1

--- a/solution.py
+++ b/solution.py
@@ -317,6 +317,219 @@
     )
 
 
+def expert_kernel(
+    stride, span, stream, normed, weight, slot, w_gate, w_up, w_down, out_ref,
+    v_gate, v_up, v_down, z_send, z_got, data, part, from_core, from_x, from_y, back_got,
+    w_sem, s_sem, r_sem,
+):
+    sp, tp = lax.axis_index("sp"), lax.axis_index("tp")
+    width = normed.shape[1]
+    half = (data.shape[1] // 32 + 1) * 16 if (data.shape[1] // 16) % 2 else data.shape[1] // 2
+    top, low = slice(0, half), slice(half, data.shape[1])
+    place, side = sp // 2, lax.rem(sp, 2)
+    core, across, along = (sp, flip_bit(tp, 1)), (sp, flip_bit(tp, 2)), (flip_bit(sp, 1), tp)
+    far = [(lax.rem(place + off, GROUPS), off) for off in range(1, GROUPS)]
+    loads = [
+        pltpu.make_async_copy(source, target, w_sem.at[i])
+        for i, (source, target) in enumerate(((w_gate, v_gate), (w_up, v_up), (w_down, v_down)))
+    ]
+    for load in loads:
+        load.start()
+    meet([(z * 2 + side, tp) for z, _ in far] + [core, across, along])
+
+    def copy(number, source, target, device):
+        return pltpu.make_async_remote_copy(
+            src_ref=source,
+            dst_ref=target,
+            send_sem=s_sem.at[number],
+            recv_sem=r_sem.at[number],
+            device_id=device,
+            device_id_type=MESH,
+        )
+
+    rows = slot.shape[1]
+    spread = (
+        lax.broadcasted_iota(jnp.int32, (GROUPS * span, rows), 0) == slot[...]
+    ).astype(jnp.float32).astype(jnp.bfloat16)
+    high = weight[...].astype(jnp.bfloat16)
+    rest = (weight[...] - high.astype(jnp.float32)).astype(jnp.bfloat16)
+    z_send[:, :width] = contract(spread, normed[...], NN).astype(jnp.bfloat16)
+    z_send[:, width : width + 128] = contract(spread, high, NN).astype(jnp.bfloat16)
+    z_send[:, width + 128 :] = contract(spread, rest, NN).astype(jnp.bfloat16)
+
+    def block(index):
+        return pl.ds(pl.multiple_of(index * span, 16), span)
+
+    def turn(index):
+        return pl.ds(pl.multiple_of(index * stride, 16), span)
+
+    outs = [copy(off, z_send.at[block(z)], z_got.at[off], (z * 2 + side, tp)) for z, off in far]
+    for one in outs:
+        one.start()
+    data[0] = jnp.zeros(data.shape[1:], jnp.bfloat16)
+    data[0, turn(place), :] = z_send[block(place), :]
+    for one, (_, off) in zip(outs, far):
+        one.wait()
+        source = lax.rem(place - off + GROUPS, GROUPS)
+        data[0, turn(source), :] = data[0, turn(source), :] + z_got[off]
+
+    base = GROUPS
+    c_0 = copy(base, data.at[0], data.at[1], core)
+    a_y = copy(base + 1, data.at[0, top], data.at[2, top], along)
+    b_x = copy(base + 2, data.at[0, low], data.at[4, low], across)
+    a_x = copy(base + 3, data.at[0, top], data.at[4, top], across)
+    b_y = copy(base + 4, data.at[0, low], data.at[2, low], along)
+    a_d = copy(base + 5, data.at[2, top], data.at[6, top], across)
+    b_d = copy(base + 6, data.at[4, low], data.at[6, low], along)
+    c_y = copy(base + 7, data.at[2], data.at[3], core)
+    c_x = copy(base + 8, data.at[4], data.at[5], core)
+    c_d = copy(base + 9, data.at[6], data.at[7], core)
+    base += 10
+    p_c = [copy(base + i, part.at[2 * i + 1], from_core.at[i], core) for i in range(4)]
+    base += 4
+    r_ax = copy(base, part.at[4, top], from_x.at[0, top], across)
+    r_by = copy(base + 1, part.at[2, low], from_y.at[0, low], along)
+    r_ad = copy(base + 2, part.at[6, top], from_x.at[1, top], across)
+    r_bd = copy(base + 3, part.at[6, low], from_y.at[1, low], along)
+    r_ay = copy(base + 4, part.at[2, top], from_y.at[0, top], along)
+    r_bx = copy(base + 5, part.at[4, low], from_x.at[0, low], across)
+    base += 6
+    for one in (a_y, b_x, a_x, b_y, c_0):
+        one.start()
+
+    for load in loads:
+        load.wait()
+
+    def compute(first, count):
+        @pl.loop(first, first + count)
+        def _(m):
+            x = data[m, :, :width]
+            w = data[m, :, width : width + 128].astype(jnp.float32) + data[
+                m, :, width + 128 :
+            ].astype(jnp.float32)
+            lane = lax.broadcasted_iota(jnp.int32, w.shape, 1)
+            w = jnp.sum(jnp.where(lane == side, w, 0.0), axis=1, keepdims=True)
+            gate = contract(x, v_gate[...], NN)
+            up = contract(x, v_up[...], NN)
+            hidden = (gate / (1.0 + jnp.exp(-gate)) * up * w).astype(jnp.bfloat16)
+            part[m] = contract(hidden, v_down[...], NN).astype(jnp.bfloat16)
+
+    def add(m, where, term):
+        part[m, where, :] = (
+            part[m, where, :].astype(jnp.float32) + term.astype(jnp.float32)
+        ).astype(jnp.bfloat16)
+
+    everything = slice(0, data.shape[1])
+    c_0.wait_recv()
+    compute(0, 2)
+    p_c[0].start()
+    a_y.wait_recv()
+    a_d.start()
+    b_x.wait_recv()
+    b_d.start()
+    b_y.wait_recv()
+    c_y.start()
+    a_x.wait_recv()
+    c_x.start()
+    c_y.wait_recv()
+    c_x.wait_recv()
+    compute(2, 4)
+    p_c[1].start()
+    p_c[2].start()
+    p_c[1].wait_recv()
+    add(2, everything, from_core[1])
+    r_by.start()
+    p_c[2].wait_recv()
+    add(4, everything, from_core[2])
+    r_ax.start()
+    a_d.wait_recv()
+    b_d.wait_recv()
+    c_d.start()
+    c_d.wait_recv()
+    compute(6, 2)
+    p_c[3].start()
+    p_c[3].wait_recv()
+    add(6, everything, from_core[3])
+    r_ad.start()
+    r_bd.start()
+    p_c[0].wait_recv()
+    r_ad.wait_recv()
+    add(2, top, from_x[1, top])
+    r_ay.start()
+    r_bd.wait_recv()
+    add(4, low, from_y[1, low])
+    r_bx.start()
+    r_ax.wait_recv()
+    r_by.wait_recv()
+    r_ay.wait_recv()
+    r_bx.wait_recv()
+    f32 = jnp.float32
+    summed = part[0].astype(f32) + from_core[0].astype(f32)
+    part[0] = (summed + from_x[0].astype(f32) + from_y[0].astype(f32)).astype(jnp.bfloat16)
+
+    outs = []
+    for z, off in far:
+        outs.append(copy(base + off, part.at[0, turn(z)], back_got.at[block(place)], (z * 2 + side, tp)))
+        outs[-1].start()
+    back_got[block(place), :] = part[0, turn(place), :]
+    for one in outs:
+        one.wait_recv()
+    picked = contract(spread, back_got[...], TN)
+    out_ref[...] = (stream[...].astype(f32) + picked).astype(jnp.bfloat16)
+    for one in [c_0, a_y, b_x, a_x, b_y, a_d, b_d, c_y, c_x, c_d] + p_c + outs:
+        one.wait_send()
+    for one in (r_ax, r_by, r_ad, r_bd, r_ay, r_bx):
+        one.wait_send()
+
+
+def grouped_experts(stream, normed, routes, weights, capacity, w_gate, w_up, w_down):
+    rows, width = stream.shape
+    stride = (capacity - 1) // 16 * 16
+    if stride + 1 < capacity:
+        stride += 16
+    span = -(-(capacity + (GROUPS - 1) * max(0, capacity - stride)) // 16) * 16
+    length = stride * (GROUPS - 1) + span
+    group = routes[:, 0] // 2
+    position = jnp.arange(rows, dtype=jnp.int32)
+    ahead = (group[:, None] == group[None, :]) & (position[None, :] < position[:, None])
+    nth = jnp.sum(ahead.astype(jnp.int32), axis=1)
+    shift = lax.axis_index("sp") // 2 * max(0, capacity - stride)
+    slot = (group * span + shift + nth)[None, :]
+    side = routes[:, :, None] % 2 == jnp.arange(128, dtype=jnp.int32)[None, None, :]
+    weight = jnp.sum(jnp.where(side, weights[:, :, None], 0.0), axis=1)
+    bf = jnp.bfloat16
+    vmem = pl.BlockSpec(memory_space=pltpu.VMEM)
+    hbm = pl.BlockSpec(memory_space=pl.ANY)
+    sem = pltpu.SemaphoreType.DMA
+    wide = width + 256
+    copies = 2 * GROUPS + 20
+    return pl.pallas_call(
+        functools.partial(expert_kernel, stride, span),
+        out_shape=jax.ShapeDtypeStruct((rows, width), bf),
+        in_specs=[vmem] * 4 + [hbm] * 3,
+        out_specs=vmem,
+        scratch_shapes=[
+            pltpu.VMEM(w_gate.shape, bf),
+            pltpu.VMEM(w_up.shape, bf),
+            pltpu.VMEM(w_down.shape, bf),
+            pltpu.VMEM((GROUPS * span, wide), bf),
+            pltpu.VMEM((GROUPS, span, wide), bf),
+            pltpu.VMEM((8, length, wide), bf),
+            pltpu.VMEM((8, length, width), bf),
+            pltpu.VMEM((4, length, width), bf),
+            pltpu.VMEM((2, length, width), bf),
+            pltpu.VMEM((2, length, width), bf),
+            pltpu.VMEM((GROUPS * span, width), bf),
+            sem((3,)),
+            sem((copies,)),
+            sem((copies,)),
+        ],
+        compiler_params=pltpu.CompilerParams(
+            collective_id=1, has_side_effects=True, vmem_limit_bytes=60 * 2**20
+        ),
+    )(stream, normed, weight, slot, w_gate, w_up, w_down)
+
+
 def slot_table(routes, capacity, experts):
     flat = routes.reshape(-1)
     count = flat.shape[0]
@@ -372,6 +585,17 @@
     own_group = lax.dynamic_slice_in_dim(group_weight, rank * rows_dev, rows_dev, 0)
     own_pair = lax.dynamic_slice_in_dim(pair_weight, rank * rows_dev, rows_dev, 0)
     weights = own_group[:, None] * own_pair / jnp.sum(own_pair, axis=1, keepdims=True)
+    if experts == 2 * GROUPS and lax.axis_size("tp") == 4:
+        return grouped_experts(
+            stream,
+            normed_rows,
+            own_routes,
+            weights,
+            capacity,
+            expert_gate[0],
+            expert_up[0],
+            expert_down[0],
+        )
     blank = jnp.zeros((1, D), jnp.bfloat16)
     table, own_place = slot_table(own_routes, capacity, experts)
     index = jnp.where(table == 2 * rows_dev, rows_dev, table // 2)

time: 324 us -> 168 us (0.52)
  waiting for transfers between devices: 153 us -> 0 us
  Pallas kernels: 42 us -> 161 us
  blocking collectives: 53.1 us -> 0 us
  local copies, waits for them, and re-layouts: 40.1 us -> 2.54 us
  between operations: 13.6 us -> 0.03 us
  matrix products: 12.1 us -> 0 us
  starting transfers between devices: 5.87 us -> 0 us
    pallas_call x0 -> x1, Pallas kernels: none -> 119 us  [grouped_experts(): pl.pallas_call(functools.partial(expert_kernel, stride, span), out_shape=...]
    reduce_scatter x1 -> x0, waiting for transfers between devices: 66.1 us -> none  [body(): lax.psum_scatter(jnp.dot(hidden, expert_down[0], preferred_element_type=j...]
    all_to_all x1 -> x0, blocking collectives: 53.1 us -> none  [body(): lax.all_to_all(send, 'sp', split_axis=1, concat_axis=1, tiled=True)]
    all_gather x1 -> x0, waiting for transfers between devices: 45.1 us -> none  [body(): received = lax.all_gather(received, 'tp', axis=0, tiled=True)]
    all_to_all x1 -> x0, waiting for transfers between devices: 41.5 us -> none  [body(): lax.all_to_all(share_sum, 'sp', split_axis=1, concat_axis=1, tiled=True)]
    dot_general x3 -> x0, matrix products: 12.1 us -> none  [the longest x1 5.05 us: body(): jnp.dot(hidden, expert_down[0], preferred_element_type=jnp.float32)]
    all_gather x1 -> x0, local copies, waits for them, and re-layouts: 9.59 us -> none  [body(): received = lax.all_gather(received, 'tp', axis=0, tiled=True)]
    scatter x1 -> x0, local copies, waits for them, and re-layouts: 9.28 us -> none  [slot_table(): table = jnp.full((experts, capacity), count, jnp.int32).at[flat, place].s...]
  transfers between devices with their start and end apart: 3 -> 0, of which waited for: 3 -> 0; matrix products, arithmetic and copies ran while one was open for 0% -> 0% of each run, Pallas kernels for 0% -> 0%
where the time goes in v2:
time: 168 us; the launch traced here: 166 us
  Pallas kernels  161 us (96%)
  local copies, waits for them, and re-layouts  2.54 us (2%)
  other arithmetic  2.45 us (1%)
    pallas_call x1, Pallas kernels, grouped_experts(): pl.pallas_call(functools.partial(expert_kernel, stride, span), out_shape=...  119 us
    pallas_call x1, Pallas kernels, mixer(): pl.pallas_call(functools.partial(mixer_kernel, n_sp, n_tp), out_shape=(ja...  42 us

profile of v2, /device:TPU:0, one launch (start us, length us, event | category | flops | bytes accessed | tf_op | source)
XLA Modules:
  0.0 166.2 jit_solution(6393609302583150026)
XLA Ops:
  0.0 0.0 copy-start
  0.0 0.8 dynamic_slice.10
  0.8 0.0 copy-done
  0.8 0.1 dynamic-slice_reduce_fusion
  0.9 0.1 multiply_divide_fusion
  0.9 0.8 and_select_fusion.3
  1.7 0.2 convert_reduce_fusion
  1.9 0.6 bitcast_add_fusion.slot
  2.5 0.7 select_reduce_fusion.weight
  3.2 42.0 %shard_map.208 = (bf16[96,2048]{1,0:T(8,128)(2,1)}, bf16[96,2048]{1,0:T(8,128)(2,1)}) custom-call(bf16[384,128]{1,0:T(8,128)(2,1)} %q1.1, bf16[384,128]{1,0:T(8,128)(2,1)} %k1.1, bf16[384,256]{1,0:T(8,128)(2,1)} %v1.1, bf16[384,256]{1,0:T(8,128)(2,1)} %g1.1, bf16[2,384,128]{2,1,0:T(8,128)(2,1)} %d1.1, bf16[384,256]{1,0:T(8,128)(2,1)} %q2.1, ...), custom_call_target="tpu_custom_call" | custom-call | tf_op jit(solution)/shard_map/pallas_call | solution.py:288
  45.3 119.2 %shard_map.209 = bf16[96,2048]{1,0:T(8,128)(2,1)} custom-call(bf16[96,2048]{1,0:T(8,128)(2,1)} %get-tuple-element.7.stream, bf16[96,2048]{1,0:T(8,128)(2,1)} %get-tuple-element.8.normed, f32[96,128]{1,0:T(8,128)} %select_reduce_fusion.weight, s32[1,96]{1,0:T(1,128)} %bitcast_add_fusion.slot, bf16[2048,256]{1,0:T(8,128)(2,1)} %bitcast.28, ...), custom_call_target="tpu_custom_call" | custom-call | tf_op jit(solution)/shard_map/pallas_call | solution.py:506
  164.4 1.8 %copy.26 = bf16[96,2048]{1,0:T(8,128)(2,1)} copy(bf16[96,2048]{1,0:T(8,128)(2,1)} %shard_map.209) | data formatting | bytes 786432
  (2 shorter events, 0.0 us)
Async XLA Ops:
  0.0 0.8 copy-start

commit v3 on v2

--- a/solution.py
+++ b/solution.py
@@ -354,8 +354,9 @@
     high = weight[...].astype(jnp.bfloat16)
     rest = (weight[...] - high.astype(jnp.float32)).astype(jnp.bfloat16)
     z_send[:, :width] = contract(spread, normed[...], NN).astype(jnp.bfloat16)
-    z_send[:, width : width + 128] = contract(spread, high, NN).astype(jnp.bfloat16)
-    z_send[:, width + 128 :] = contract(spread, rest, NN).astype(jnp.bfloat16)
+    second = lax.broadcasted_iota(jnp.int32, high.shape, 1) >= 64
+    both = jnp.where(second, rest.astype(jnp.float32), high.astype(jnp.float32))
+    z_send[:, width:] = contract(spread, both.astype(jnp.bfloat16), NN).astype(jnp.bfloat16)
 
     def block(index):
         return pl.ds(pl.multiple_of(index * span, 16), span)
@@ -404,11 +405,9 @@
         @pl.loop(first, first + count)
         def _(m):
             x = data[m, :, :width]
-            w = data[m, :, width : width + 128].astype(jnp.float32) + data[
-                m, :, width + 128 :
-            ].astype(jnp.float32)
+            w = data[m, :, width:].astype(jnp.float32)
             lane = lax.broadcasted_iota(jnp.int32, w.shape, 1)
-            w = jnp.sum(jnp.where(lane == side, w, 0.0), axis=1, keepdims=True)
+            w = jnp.sum(jnp.where((lane == side) | (lane == side + 64), w, 0.0), axis=1, keepdims=True)
             gate = contract(x, v_gate[...], NN)
             up = contract(x, v_up[...], NN)
             hidden = (gate / (1.0 + jnp.exp(-gate)) * up * w).astype(jnp.bfloat16)
@@ -445,8 +444,9 @@
     a_d.wait_recv()
     b_d.wait_recv()
     c_d.start()
+    compute(6, 1)
     c_d.wait_recv()
-    compute(6, 2)
+    compute(7, 1)
     p_c[3].start()
     p_c[3].wait_recv()
     add(6, everything, from_core[3])
@@ -495,13 +495,13 @@
     nth = jnp.sum(ahead.astype(jnp.int32), axis=1)
     shift = lax.axis_index("sp") // 2 * max(0, capacity - stride)
     slot = (group * span + shift + nth)[None, :]
-    side = routes[:, :, None] % 2 == jnp.arange(128, dtype=jnp.int32)[None, None, :]
+    side = routes[:, :, None] % 2 == (jnp.arange(128, dtype=jnp.int32) % 64)[None, None, :]
     weight = jnp.sum(jnp.where(side, weights[:, :, None], 0.0), axis=1)
     bf = jnp.bfloat16
     vmem = pl.BlockSpec(memory_space=pltpu.VMEM)
     hbm = pl.BlockSpec(memory_space=pl.ANY)
     sem = pltpu.SemaphoreType.DMA
-    wide = width + 256
+    wide = width + 128
     copies = 2 * GROUPS + 20
     return pl.pallas_call(
         functools.partial(expert_kernel, stride, span),

time: 168 us -> 164 us (0.976)
  Pallas kernels: 161 us -> 156 us
    pallas_call x1, Pallas kernels: 119 us -> 114 us  [grouped_experts(): pl.pallas_call(functools.partial(expert_kernel, stride, span), out_shape=...]
where the time goes in v3:
time: 164 us; the launch traced here: 161 us
  Pallas kernels  156 us (95%)
  local copies, waits for them, and re-layouts  2.54 us (2%)
  other arithmetic  2.46 us (2%)
    pallas_call x1, Pallas kernels, grouped_experts(): pl.pallas_call(functools.partial(expert_kernel, stride, span), out_shape=...  114 us
    pallas_call x1, Pallas kernels, mixer(): pl.pallas_call(functools.partial(mixer_kernel, n_sp, n_tp), out_shape=(ja...  42.2 us

profile of v3, /device:TPU:0, one launch (start us, length us, event | category | flops | bytes accessed | tf_op | source)
XLA Modules:
  0.0 161.0 jit_solution(659832214187288711)
XLA Ops:
  0.0 0.0 copy-start
  0.0 0.8 dynamic_slice.10
  0.8 0.0 copy-done
  0.8 0.1 dynamic-slice_reduce_fusion
  0.9 0.1 multiply_divide_fusion
  0.9 0.8 and_select_fusion.4
  1.7 0.2 convert_reduce_fusion
  1.9 0.6 bitcast_add_fusion.slot
  2.5 0.7 select_reduce_fusion.weight
  3.2 42.2 %shard_map.208 = (bf16[96,2048]{1,0:T(8,128)(2,1)}, bf16[96,2048]{1,0:T(8,128)(2,1)}) custom-call(bf16[384,128]{1,0:T(8,128)(2,1)} %q1.1, bf16[384,128]{1,0:T(8,128)(2,1)} %k1.1, bf16[384,256]{1,0:T(8,128)(2,1)} %v1.1, bf16[384,256]{1,0:T(8,128)(2,1)} %g1.1, bf16[2,384,128]{2,1,0:T(8,128)(2,1)} %d1.1, bf16[384,256]{1,0:T(8,128)(2,1)} %q2.1, ...), custom_call_target="tpu_custom_call" | custom-call | tf_op jit(solution)/shard_map/pallas_call | solution.py:288
  45.4 113.7 %shard_map.209 = bf16[96,2048]{1,0:T(8,128)(2,1)} custom-call(bf16[96,2048]{1,0:T(8,128)(2,1)} %get-tuple-element.7.stream, bf16[96,2048]{1,0:T(8,128)(2,1)} %get-tuple-element.8.normed, f32[96,128]{1,0:T(8,128)} %select_reduce_fusion.weight, s32[1,96]{1,0:T(1,128)} %bitcast_add_fusion.slot, bf16[2048,256]{1,0:T(8,128)(2,1)} %bitcast.28, ...), custom_call_target="tpu_custom_call" | custom-call | tf_op jit(solution)/shard_map/pallas_call | solution.py:506
  159.2 1.8 %copy.26 = bf16[96,2048]{1,0:T(8,128)(2,1)} copy(bf16[96,2048]{1,0:T(8,128)(2,1)} %shard_map.209) | data formatting | bytes 786432
  (3 shorter events, 0.0 us)
Async XLA Ops:
  0.0 0.8 copy-start
